TPU v7x, 32 devices: a whole 2x2x4 slice. The times are simulated.
32 devices in a mesh: fs: 8 (over z, y), tp: 4 (over x, core).
Axes of the slice: x: 2, y: 2, z: 4, core: 2. Of those that a mesh axis runs over, the one named last changes fastest.
Arguments:
- tokens: bfloat16 [4096, 2048], P(('fs', 'tp')), may hold values from -6 to 6
- routes: int32 [4096, 4], P(('fs', 'tp')), may hold values from 0 to 31, all different within a row; in each aligned block of 128 rows (0 to 127, 128 to 255, ...) at most 24 rows name the same one
- route_weight: float32 [4096, 4], P(('fs', 'tp')), may hold values from 0.1 to 1
- norm_gain: float32 [2048], P('fs'), may hold values from 0.5 to 4
- gate_weight: float32 [32, 2048, 512], P(None, 'fs', 'tp'), may hold values from -0.125 to 0.125
- up_weight: float32 [32, 2048, 512], P(None, 'fs', 'tp'), may hold values from -0.125 to 0.125
- down_weight: float32 [32, 512, 2048], P(None, 'fs', 'tp'), may hold values from -0.0625 to 0.0625
Outputs:
- gate_new: bfloat16 [32, 2048, 512], P(('fs', 'tp'))
- up_new: bfloat16 [32, 2048, 512], P(('fs', 'tp'))
- down_new: bfloat16 [32, 512, 2048], P(('fs', 'tp'))
- mixed: bfloat16 [4096, 2048], P(('fs', 'tp'))
Inputs may be any that keep to these rules, and one draw needn't show every extreme that they name: `routes`: each row names 4 different experts, and every expert is named by some row; within the 128 rows of one device no expert is named by more than 24 rows, and in some blocks an expert is named by exactly 24 rows.
All inputs are finite; a program needn't handle non-finite values.
Results may differ from a plain program's by a relative error of at most 0.0084.
Values may be sent and summed in bfloat16 or wider, within the bound.
A program may use at most 128 MiB of HBM per device.

v0:
```python
import jax
import jax.numpy as jnp
from jax import lax
from jax.sharding import PartitionSpec as P

norm_epsilon = 1e-06
clamp_limit = 7.0
sigmoid_slope = 1.702


def feed(inputs, gate_mat, up_mat, down_mat):
    gate_pre = jnp.dot(inputs, gate_mat, preferred_element_type=jnp.float32)
    up_pre = jnp.dot(inputs, up_mat, preferred_element_type=jnp.float32)
    gate_part = jnp.minimum(gate_pre, clamp_limit)
    linear_part = jnp.clip(up_pre, -clamp_limit, clamp_limit)
    activation = (
        gate_part * jax.nn.sigmoid(sigmoid_slope * gate_part) * (linear_part + 1.0)
    ).astype(jnp.bfloat16)
    return jnp.dot(activation, down_mat, preferred_element_type=jnp.float32).astype(jnp.bfloat16)


def assemble(received, rows_groups, column_groups):
    tile_rows = received.shape[2]
    tile_columns = received.shape[3]
    sources = received.reshape(rows_groups, column_groups, tile_rows, tile_columns)
    return sources.transpose(0, 2, 1, 3).reshape(
        1, rows_groups * tile_rows, column_groups * tile_columns
    )


def shards(tokens, routes, route_weight, norm_gain, gate_weight, up_weight, down_weight):
    gain_column = norm_gain[None, :, None]
    gate_tiles = (gate_weight * gain_column).astype(jnp.bfloat16)
    up_tiles = (up_weight * gain_column).astype(jnp.bfloat16)
    down_tiles = down_weight.astype(jnp.bfloat16)
    rows_groups = lax.axis_size("fs")
    column_groups = lax.axis_size("tp")
    arrived = (
        lax.all_to_all(gate_tiles[:, None], ("fs", "tp"), split_axis=0, concat_axis=1, tiled=True),
        lax.all_to_all(up_tiles[:, None], ("fs", "tp"), split_axis=0, concat_axis=1, tiled=True),
        lax.all_to_all(down_tiles[:, None], ("fs", "tp"), split_axis=0, concat_axis=1, tiled=True),
    )
    gate_new = assemble(arrived[0], rows_groups, column_groups)
    up_new = assemble(arrived[1], rows_groups, column_groups)
    down_new = assemble(arrived[2], rows_groups, column_groups)
    experts = rows_groups * column_groups
    tok_rows, model_width = tokens.shape
    per_token = routes.shape[1]
    capacity = max(2, 3 * tok_rows * per_token // (2 * experts))
    values = tokens.astype(jnp.float32)
    squares = jnp.mean(values * values, axis=1, keepdims=True)
    normed = (values * lax.rsqrt(squares + norm_epsilon)).astype(jnp.bfloat16)
    flat_routes = routes.reshape(-1)
    onehot = (flat_routes[:, None] == jnp.arange(experts, dtype=jnp.int32)[None, :]).astype(
        jnp.int32
    )
    earlier = jnp.cumsum(onehot, axis=0) - onehot
    rank = jnp.sum(earlier * onehot, axis=1)
    slot_index = flat_routes * capacity + rank
    slot_numbers = jnp.arange(experts * capacity, dtype=jnp.int32)
    select = jnp.any(
        slot_index.reshape(tok_rows, per_token)[None, :, :] == slot_numbers[:, None, None], axis=2
    )
    buffer = jnp.dot(
        select.astype(jnp.bfloat16), normed, preferred_element_type=jnp.float32
    ).astype(jnp.bfloat16)
    buffer = buffer.reshape(experts, 1, capacity, model_width)
    slot_rows = lax.all_to_all(buffer, ("fs", "tp"), split_axis=0, concat_axis=1, tiled=True)
    sources = slot_rows.shape[1]
    count = slot_rows.shape[2]
    expert_out = feed(slot_rows.reshape(-1, model_width), gate_new[0], up_new[0], down_new[0])
    expert_out = expert_out.reshape(1, sources, count, model_width)
    returned = lax.all_to_all(expert_out, ("fs", "tp"), split_axis=1, concat_axis=0, tiled=True)
    returned = returned.reshape(experts * capacity, model_width)
    picked = returned[slot_index].reshape(tok_rows, per_token, model_width)
    mixed = jnp.sum(picked.astype(jnp.float32) * route_weight[:, :, None], axis=1).astype(
        jnp.bfloat16
    )
    return (gate_new, up_new, down_new, mixed)


def solution(mesh):
    placed = (
        P(("fs", "tp"), None),
        P(("fs", "tp"), None),
        P(("fs", "tp"), None),
        P("fs"),
        P(None, "fs", "tp"),
        P(None, "fs", "tp"),
        P(None, "fs", "tp"),
    )
    return jax.shard_map(
        shards,
        mesh=mesh,
        in_specs=placed,
        out_specs=(
            P(("fs", "tp"), None, None),
            P(("fs", "tp"), None, None),
            P(("fs", "tp"), None, None),
            P(("fs", "tp"), None),
        ),
        check_vma=False,
    )
```

profile of v0, /device:TPU:0, one launch (start us, length us, event | category | flops | bytes accessed | tf_op | source)
XLA Modules:
  0.0 347.1 jit_solution(5978215491668474346)
XLA Ops:
  0.6 6.0 %fusion.1 = (bf16[32,1,256,128]{3,2,1,0:T(8,128)(2,1)}, bf16[32,1,256,128]{3,2,1,0:T(8,128)(2,1)S(1)}) fusion(f32[32,256,128]{2,1,0:T(8,128)} %param.12, f32[256]{0:T(256)} %param.10, f32[32,256,128]{2,1,0:T(8,128)} %param.11), kind=kLoop, calls=%fused_computation.7 | loop fusion | flops 4194304 | bytes 12583936 | tf_op jit(solution)/shard_map/broadcast_in_dim | solution.py:40
  6.6 55.9 %all_to_all.20 = bf16[32,1,256,128]{3,2,1,0:T(8,128)(2,1)} all-to-all(bf16[32,1,256,128]{3,2,1,0:T(8,128)(2,1)S(1)} %get-tuple-element.9), channel_id=1, replica_groups=mesh['fs'=8,'tp'=4] {'fs','tp'}, dimensions={0} | all-to-all | bytes 4194304 | tf_op jit(solution)/shard_map/all_to_all | solution.py:39
  62.5 3.7 %all-to-all-start.1 = ((bf16[32,1,256,128]{3,2,1,0:T(8,128)(2,1)}), bf16[32,1,256,128]{3,2,1,0:T(8,128)(2,1)S(1)}, u32[]{:S(2)}, u32[]{:S(2)}) async-start(bf16[32,1,256,128]{3,2,1,0:T(8,128)(2,1)} %get-tuple-element.8), calls=%async_computation.1 | async-start | bytes 4194304 | tf_op jit(solution)/shard_map/all_to_all | solution.py:40
  66.2 3.8 %convert_bitcast_fusion = bf16[32,1,64,512]{3,2,1,0:T(8,128)(2,1)} fusion(f32[32,64,512]{2,1,0:T(8,128)} %param.13), kind=kLoop, calls=%fused_computation.8 | loop fusion | flops 1048576 | bytes 6291456 | tf_op jit(solution)/shard_map/broadcast_in_dim | solution.py:41
  70.0 0.0 copy-start.4
  70.0 44.9 %all-to-all-done.1 = bf16[32,1,256,128]{3,2,1,0:T(8,128)(2,1)S(1)} async-done(((bf16[32,1,256,128]{3,2,1,0:T(8,128)(2,1)}), bf16[32,1,256,128]{3,2,1,0:T(8,128)(2,1)S(1)}, u32[]{:S(2)}, u32[]{:S(2)}) %all-to-all-start.1) | async-done | bytes 2097184 | tf_op jit(solution)/shard_map/all_to_all | solution.py:40
  114.9 4.2 %all-to-all-start.2 = ((bf16[32,1,64,512]{3,2,1,0:T(8,128)(2,1)}), bf16[32,1,64,512]{3,2,1,0:T(8,128)(2,1)}, u32[]{:S(2)}, u32[]{:S(2)}) async-start(bf16[32,1,64,512]{3,2,1,0:T(8,128)(2,1)} %convert_bitcast_fusion), calls=%async_computation.2 | async-start | bytes 4194304 | tf_op jit(solution)/shard_map/all_to_all | solution.py:41
  119.1 0.0 copy-done.4
  119.1 0.1 copy.54
  119.3 0.1 eq.42
  119.4 0.1 eq.38
  119.5 1.2 reduce-window.6
  120.7 0.2 slice_reduce_fusion
  120.9 0.1 fusion.9
  121.0 0.1 reduce_sum.32
  121.2 0.1 copy.58
  121.2 0.2 fusion.2
  121.5 0.0 copy-done.3
  121.5 0.2 fusion.3
  121.7 2.8 convolution_convert_fusion.1
  124.4 43.4 %all-to-all-done.2 = bf16[32,1,64,512]{3,2,1,0:T(8,128)(2,1)} async-done(((bf16[32,1,64,512]{3,2,1,0:T(8,128)(2,1)}), bf16[32,1,64,512]{3,2,1,0:T(8,128)(2,1)}, u32[]{:S(2)}, u32[]{:S(2)}) %all-to-all-start.2) | async-done | bytes 2097184 | tf_op jit(solution)/shard_map/all_to_all | solution.py:41
  167.8 4.4 %all-to-all-start.3 = ((bf16[32,1,24,2048]{3,2,1,0:T(8,128)(2,1)}), bf16[32,1,24,2048]{3,2,1,0:T(8,128)(2,1)}, u32[]{:S(2)}, u32[]{:S(2)}) async-start(bf16[32,1,24,2048]{3,2,1,0:T(8,128)(2,1)} %bitcast.74), calls=%async_computation.3 | async-start | bytes 6291456 | tf_op jit(solution)/shard_map/all_to_all | solution.py:68
  172.2 4.5 %copy.48 = bf16[8,4,256,128]{2,0,3,1:T(8,128)(2,1)} copy(bf16[8,4,256,128]{3,2,1,0:T(8,128)(2,1)} %bitcast.70) | data formatting | bytes 4194304 | tf_op jit(solution)/shard_map/reshape | solution.py:25
  176.7 3.6 %copy.65 = bf16[64,8,8,256]{3,1,2,0:T(8,128)(2,1)} copy(bf16[64,8,8,256]{3,2,1,0:T(8,128)(2,1)} %bitcast.75) | data formatting | bytes 4194304
  180.3 0.0 copy-done
  180.3 2.9 copy.51
  183.2 3.6 %copy.66 = bf16[64,8,8,256]{3,1,2,0:T(8,128)(2,1)} copy(bf16[64,8,8,256]{3,2,1,0:T(8,128)(2,1)} %bitcast.76) | data formatting | bytes 4194304
  186.8 3.2 copy.71
  190.0 0.0 copy-start.1
  190.0 1.4 copy-done.1
  191.4 2.0 copy.67
  193.4 50.1 %all-to-all-done.3 = bf16[32,1,24,2048]{3,2,1,0:T(8,128)(2,1)} async-done(((bf16[32,1,24,2048]{3,2,1,0:T(8,128)(2,1)}), bf16[32,1,24,2048]{3,2,1,0:T(8,128)(2,1)}, u32[]{:S(2)}, u32[]{:S(2)}) %all-to-all-start.3) | async-done | bytes 3145760 | tf_op jit(solution)/shard_map/all_to_all | solution.py:68
  243.5 0.0 copy-done.2
  243.5 4.9 %fusion.17 = f32[768,512]{1,0:T(8,128)} fusion(bf16[768,2048]{1,0:T(8,128)(2,1)} %bitcast.15, bf16[2048,512]{0,1:T(8,128)(2,1)S(1)} %bitcast.78), kind=kOutput, calls=%fused_computation.37 | convolution fusion | flops 1610612736 | bytes 6815744 | tf_op jit(solution)/shard_map/dot_general | solution.py:12
  248.3 9.0 %convolution_convert_fusion = bf16[768,2048]{1,0:T(8,128)(2,1)} fusion(bf16[512,2048]{1,0:T(8,128)(2,1)} %bitcast.80, f32[768,512]{1,0:T(8,128)} %fusion.17, bf16[768,2048]{1,0:T(8,128)(2,1)} %bitcast.15, bf16[2048,512]{0,1:T(8,128)(2,1)} %bitcast.79), kind=kOutput, calls=%fused_computation.4 | convolution fusion | flops 3226730496 | bytes 12058624 | tf_op jit(solution)/shard_map/dot_general | solution.py:19
  257.4 4.1 %all-to-all-start.4 = ((bf16[1,32,24,2048]{3,2,0,1:T(8,128)(2,1)}), bf16[1,32,24,2048]{3,2,0,1:T(8,128)(2,1)S(1)}, u32[]{:S(2)}, u32[]{:S(2)}) async-start(bf16[1,32,24,2048]{3,2,0,1:T(8,128)(2,1)} %bitcast.77), calls=%async_computation.4 | async-start | bytes 6291456 | tf_op jit(solution)/shard_map/all_to_all | solution.py:73
  261.5 0.1 mul.79
  261.6 0.0 copy-done.5
  261.7 0.1 copy.61
  261.8 4.5 %copy.49 = bf16[8,256,4,128]{3,2,1,0:T(4,128)(2,1)} copy(bf16[8,256,4,128]{3,1,2,0:T(8,128)(2,1)} %bitcast.71) | data formatting | bytes 4194304 | tf_op jit(solution)/shard_map/transpose | solution.py:26
  266.3 4.1 %reshape.124 = bf16[1,2048,512]{2,1,0:T(8,128)(2,1)} reshape(bf16[8,256,4,128]{3,2,1,0:T(4,128)(2,1)} %copy.49) | data formatting | bytes 4194304 | tf_op jit(solution)/shard_map/reshape | solution.py:26
  270.4 4.5 %copy.52 = bf16[8,256,4,128]{3,2,1,0:T(4,128)(2,1)} copy(bf16[8,256,4,128]{3,1,2,0:T(8,128)(2,1)} %bitcast.69) | data formatting | bytes 4194304 | tf_op jit(solution)/shard_map/transpose | solution.py:26
  275.0 4.1 %reshape.126 = bf16[1,2048,512]{2,1,0:T(8,128)(2,1)} reshape(bf16[8,256,4,128]{3,2,1,0:T(4,128)(2,1)} %copy.52) | data formatting | bytes 4194304 | tf_op jit(solution)/shard_map/reshape | solution.py:26
  279.1 4.4 %reshape.128 = bf16[1,512,2048]{2,1,0:T(8,128)(2,1)} reshape(bf16[8,64,4,512]{3,2,1,0:T(4,128)(2,1)} %bitcast.73) | data formatting | bytes 4194304 | tf_op jit(solution)/shard_map/reshape | solution.py:26
  283.5 49.3 %all-to-all-done.4 = bf16[1,32,24,2048]{3,2,0,1:T(8,128)(2,1)S(1)} async-done(((bf16[1,32,24,2048]{3,2,0,1:T(8,128)(2,1)}), bf16[1,32,24,2048]{3,2,0,1:T(8,128)(2,1)S(1)}, u32[]{:S(2)}, u32[]{:S(2)}) %all-to-all-start.4) | async-done | bytes 3145760 | tf_op jit(solution)/shard_map/all_to_all | solution.py:73
  332.8 3.3 gather_fusion
  336.1 4.8 %reshape.134 = f32[128,4,2048]{2,1,0:T(4,128)} reshape(bf16[512,2048]{1,0:T(8,128)(2,1)} %gather_fusion) | data formatting | bytes 6291456 | tf_op jit(solution)/shard_map/convert_element_type | solution.py:76
  340.9 6.2 %multiply_reduce_fusion = bf16[128,2048]{1,0:T(8,128)(2,1)} fusion(f32[128,4,2048]{2,1,0:T(4,128)} %reshape.134, f32[128,4]{1,0:T(8,128)S(1)} %copy.61), kind=kLoop, calls=%fused_computation.1 | loop fusion | flops 1835008 | bytes 4720640 | tf_op jit(solution)/shard_map/reduce_sum | solution.py:76
  (11 shorter events, 0.1 us)
Async XLA Ops:
  62.5 52.4 %all-to-all-start.1 = ((bf16[32,1,256,128]{3,2,1,0:T(8,128)(2,1)}), bf16[32,1,256,128]{3,2,1,0:T(8,128)(2,1)S(1)}, u32[]{:S(2)}, u32[]{:S(2)}) async-start(bf16[32,1,256,128]{3,2,1,0:T(8,128)(2,1)} %get-tuple-element.8), calls=%async_computation.1 | async-start | bytes 4194304 | tf_op jit(solution)/shard_map/all_to_all | solution.py:40
  70.0 49.1 %copy-start.4 = (s32[128,4]{0,1:T(4,128)S(1)}, s32[128,4]{0,1:T(4,128)}, u32[]{:S(2)}) copy-start(s32[128,4]{0,1:T(4,128)} %param.8) | copy-start | bytes 6148
  70.0 51.5 %copy-start.3 = (bf16[128,2048]{1,0:T(8,128)(2,1)S(1)}, bf16[128,2048]{1,0:T(8,128)(2,1)}, u32[]{:S(2)}) copy-start(bf16[128,2048]{1,0:T(8,128)(2,1)} %param.7) | copy-start | bytes 1572868
  114.9 65.4 %copy-start = (bf16[32,1,256,128]{3,2,1,0:T(8,128)(2,1)}, bf16[32,1,256,128]{3,2,1,0:T(8,128)(2,1)S(1)}, u32[]{:S(2)}) copy-start(bf16[32,1,256,128]{3,2,1,0:T(8,128)(2,1)S(1)} %all-to-all-done.1) | copy-start | bytes 6291460
  114.9 52.9 %all-to-all-start.2 = ((bf16[32,1,64,512]{3,2,1,0:T(8,128)(2,1)}), bf16[32,1,64,512]{3,2,1,0:T(8,128)(2,1)}, u32[]{:S(2)}, u32[]{:S(2)}) async-start(bf16[32,1,64,512]{3,2,1,0:T(8,128)(2,1)} %convert_bitcast_fusion), calls=%async_computation.2 | async-start | bytes 4194304 | tf_op jit(solution)/shard_map/all_to_all | solution.py:41
  167.8 75.6 %all-to-all-start.3 = ((bf16[32,1,24,2048]{3,2,1,0:T(8,128)(2,1)}), bf16[32,1,24,2048]{3,2,1,0:T(8,128)(2,1)}, u32[]{:S(2)}, u32[]{:S(2)}) async-start(bf16[32,1,24,2048]{3,2,1,0:T(8,128)(2,1)} %bitcast.74), calls=%async_computation.3 | async-start | bytes 6291456 | tf_op jit(solution)/shard_map/all_to_all | solution.py:68
  190.0 1.4 copy-start.1
  191.4 52.1 %copy-start.2 = (bf16[64,8,8,256]{3,1,2,0:T(8,128)(2,1)S(1)}, bf16[64,8,8,256]{3,1,2,0:T(8,128)(2,1)}, u32[]{:S(2)}) copy-start(bf16[64,8,8,256]{3,1,2,0:T(8,128)(2,1)} %copy.65) | copy-start | bytes 6291460
  257.4 4.3 %copy-start.5 = (f32[128,4]{0,1:T(4,128)S(1)}, f32[128,4]{0,1:T(4,128)}, u32[]{:S(2)}) copy-start(f32[128,4]{0,1:T(4,128)} %param.9) | copy-start | bytes 6148
  257.4 75.4 %all-to-all-start.4 = ((bf16[1,32,24,2048]{3,2,0,1:T(8,128)(2,1)}), bf16[1,32,24,2048]{3,2,0,1:T(8,128)(2,1)S(1)}, u32[]{:S(2)}, u32[]{:S(2)}) async-start(bf16[1,32,24,2048]{3,2,0,1:T(8,128)(2,1)} %bitcast.77), calls=%async_computation.4 | async-start | bytes 6291456 | tf_op jit(solution)/shard_map/all_to_all | solution.py:73
where the time goes:
time: 348 us; the launch traced here: 347 us
  waiting for transfers between devices  188 us (54%)
  blocking collectives  55.9 us (16%)
  local copies, waits for them, and re-layouts  51.9 us (15%)
  other arithmetic  17.8 us (5%)
  matrix products  16.7 us (5%)
  starting transfers between devices  16.4 us (5%)
    all_to_all x1, blocking collectives, shards(): lax.all_to_all(gate_tiles[:, None], ('fs', 'tp'), split_axis=0, concat_ax...  55.9 us
    all_to_all x1, waiting for transfers between devices, shards(): lax.all_to_all(buffer, ('fs', 'tp'), split_axis=0, concat_axis=1, tiled=T...  50.1 us
    all_to_all x1, waiting for transfers between devices, shards(): lax.all_to_all(expert_out, ('fs', 'tp'), split_axis=1, concat_axis=0, til...  49.3 us
    all_to_all x1, waiting for transfers between devices, shards(): lax.all_to_all(up_tiles[:, None], ('fs', 'tp'), split_axis=0, concat_axis...  44.9 us
    all_to_all x1, waiting for transfers between devices, shards(): lax.all_to_all(down_tiles[:, None], ('fs', 'tp'), split_axis=0, concat_ax...  43.4 us
    reshape x3, local copies, waits for them, and re-layouts, assemble(): sources.transpose(0, 2, 1, 3)  12.6 us
    unnamed x17, local copies, waits for them, and re-layouts  10.7 us
    reshape x3, local copies, waits for them, and re-layouts, assemble(): received.reshape(rows_groups, column_groups, tile_rows, tile_columns)  10.6 us
  transfers between devices with their start and end apart: 4, of which 4 were waited for; matrix products, arithmetic and copies ran while one was open for 15% of the time, Pallas kernels for 0%

commit v1 on v0

--- a/solution.py
+++ b/solution.py
@@ -1,11 +1,16 @@
+import functools
+
 import jax
 import jax.numpy as jnp
 from jax import lax
+from jax.experimental import pallas as pl
+from jax.experimental.pallas import tpu as pltpu
 from jax.sharding import PartitionSpec as P
 
 norm_epsilon = 1e-06
 clamp_limit = 7.0
 sigmoid_slope = 1.702
+MESH = pl.DeviceIdType.MESH
 
 
 def feed(inputs, gate_mat, up_mat, down_mat):
@@ -79,6 +84,357 @@
     return (gate_new, up_new, down_new, mixed)
 
 
+def exchange_kernel(
+    sizes, tokens, routes_t, weight_t, gain, gate, up, down,
+    gate_out, up_out, down_out, mixed,
+    gate_in, up_in, down_in, in_tiles, out_tiles, in_mats, out_mat,
+    slots_out, slots_in, active, ranks, picks, mix_high, mix_low, rows_out, rows_in,
+    load_sem, store_sem, slot_send, slot_recv, first_send, first_recv,
+    second_send, second_recv, back_send, back_recv,
+):
+    n_fs, n_tp, capacity = sizes
+    n = n_fs * n_tp
+    fs, tp = lax.axis_index("fs"), lax.axis_index("tp")
+    me = fs * n_tp + tp
+    tok_rows, width = tokens.shape
+    tile_rows, tile_cols = gate_in.shape[1:]
+    down_rows, down_cols = down_in.shape[1:]
+    group = 8
+    groups = n // group
+    group_rows = group * capacity
+
+    def peer(step):
+        to_fs = lax.rem(fs + step // n_tp, n_fs)
+        to_tp = lax.rem(tp + lax.rem(step, n_tp), n_tp)
+        return to_fs, to_tp, to_fs * n_tp + to_tp
+
+    barrier = pltpu.get_barrier_semaphore()
+
+    def greet(step, carry):
+        to_fs, to_tp, _ = peer(step)
+        pl.semaphore_signal(barrier, inc=1, device_id=(to_fs, to_tp), device_id_type=MESH)
+        return carry
+
+    loads = [
+        pltpu.make_async_copy(gate, gate_in, load_sem.at[0]),
+        pltpu.make_async_copy(up, up_in, load_sem.at[1]),
+        pltpu.make_async_copy(down, down_in, load_sem.at[2]),
+    ]
+    for load in loads:
+        load.start()
+    lax.fori_loop(1, n, greet, 0)
+
+    experts = lax.broadcasted_iota(jnp.int32, (n, tok_rows), 0)
+    named = jnp.zeros((n, tok_rows), jnp.float32)
+    scaled = jnp.zeros((n, tok_rows), jnp.float32)
+    for k in range(routes_t.shape[0]):
+        hit = routes_t[k : k + 1, :] == experts
+        named = named + hit.astype(jnp.float32)
+        scaled = scaled + jnp.where(hit, weight_t[k : k + 1, :], 0.0)
+    before = (
+        lax.broadcasted_iota(jnp.int32, (tok_rows, tok_rows), 0)
+        < lax.broadcasted_iota(jnp.int32, (tok_rows, tok_rows), 1)
+    ).astype(jnp.float32).astype(jnp.bfloat16)
+    rank = jnp.dot(named.astype(jnp.bfloat16), before, preferred_element_type=jnp.float32)
+    ranks[...] = jnp.where(named > 0.5, rank, -1.0)
+    values = tokens[...].astype(jnp.float32)
+    squares = jnp.mean(values * values, axis=1, keepdims=True)
+    normed = (values * lax.rsqrt(squares + norm_epsilon)).astype(jnp.bfloat16)
+    for g in range(groups):
+        held = slice(g * group, (g + 1) * group)
+        number = lax.broadcasted_iota(jnp.int32, (group, capacity, tok_rows), 1).astype(jnp.float32)
+        select = (ranks[held, :][:, None, :] == number).astype(jnp.float32)
+        picks[g * group_rows : (g + 1) * group_rows, :] = (
+            select * scaled[held, :][:, None, :]
+        ).reshape(group_rows, tok_rows)
+        rows = jnp.dot(
+            select.reshape(group_rows, tok_rows).astype(jnp.bfloat16),
+            normed,
+            preferred_element_type=jnp.float32,
+        )
+        slots_out[held] = rows.reshape(group, capacity, width).astype(jnp.bfloat16)
+
+    pl.semaphore_wait(barrier, n - 1)
+
+    def slot_copy(to, source):
+        return pltpu.make_async_remote_copy(
+            src_ref=slots_out.at[to[2]],
+            dst_ref=slots_in.at[source],
+            send_sem=slot_send.at[to[2]],
+            recv_sem=slot_recv.at[source],
+            device_id=(to[0], to[1]),
+            device_id_type=MESH,
+        )
+
+    def first_copy(to, place):
+        return pltpu.make_async_remote_copy(
+            src_ref=in_tiles.at[to[2]],
+            dst_ref=in_mats.at[
+                :,
+                pl.ds(pl.multiple_of(place[0] * tile_rows, tile_rows), tile_rows),
+                pl.ds(pl.multiple_of(place[1] * tile_cols, tile_cols), tile_cols),
+            ],
+            send_sem=first_send.at[to[2]],
+            recv_sem=first_recv.at[place[2]],
+            device_id=(to[0], to[1]),
+            device_id_type=MESH,
+        )
+
+    def second_copy(to, place):
+        return pltpu.make_async_remote_copy(
+            src_ref=out_tiles.at[to[2]],
+            dst_ref=out_mat.at[
+                pl.ds(pl.multiple_of(place[0] * down_rows, down_rows), down_rows),
+                pl.ds(pl.multiple_of(place[1] * down_cols, down_cols), down_cols),
+            ],
+            send_sem=second_send.at[to[2]],
+            recv_sem=second_recv.at[place[2]],
+            device_id=(to[0], to[1]),
+            device_id_type=MESH,
+        )
+
+    def back_copy(to, source):
+        return pltpu.make_async_remote_copy(
+            src_ref=rows_out.at[to[2]],
+            dst_ref=rows_in.at[source],
+            send_sem=back_send.at[to[2]],
+            recv_sem=back_recv.at[source],
+            device_id=(to[0], to[1]),
+            device_id_type=MESH,
+        )
+
+    mine = (fs, tp, me)
+
+    def send_slots(step, carry):
+        slot_copy(peer(step), me).start()
+        return carry
+
+    lax.fori_loop(1, n, send_slots, 0)
+    slots_in[me] = slots_out[me]
+
+    loads[0].wait()
+    loads[1].wait()
+    gains = jnp.broadcast_to(gain[...], (tile_rows, tile_cols))
+
+    def cast_first(step):
+        e = peer(step)[2]
+        in_tiles[e, 0] = (gate_in[e] * gains).astype(jnp.bfloat16)
+        in_tiles[e, 1] = (up_in[e] * gains).astype(jnp.bfloat16)
+
+    cast_first(1)
+
+    def send_first(step, carry):
+        cast_first(step + 1)
+        first_copy(peer(step), mine).start()
+        return carry
+
+    lax.fori_loop(1, n, send_first, 0)
+    own_rows = pl.ds(pl.multiple_of(fs * tile_rows, tile_rows), tile_rows)
+    own_cols = pl.ds(pl.multiple_of(tp * tile_cols, tile_cols), tile_cols)
+    in_mats[0, own_rows, own_cols] = in_tiles[me, 0]
+    in_mats[1, own_rows, own_cols] = in_tiles[me, 1]
+
+    loads[2].wait()
+
+    def cast_second(step):
+        e = peer(step)[2]
+        out_tiles[e] = down_in[e].astype(jnp.bfloat16)
+
+    cast_second(1)
+
+    def send_second(step, carry):
+        cast_second(step + 1)
+        second_copy(peer(step), mine).start()
+        return carry
+
+    lax.fori_loop(1, n, send_second, 0)
+    out_mat[
+        pl.ds(pl.multiple_of(fs * down_rows, down_rows), down_rows),
+        pl.ds(pl.multiple_of(tp * down_cols, down_cols), down_cols),
+    ] = out_tiles[me]
+
+    shares = jnp.transpose(picks[...])
+    high = shares.astype(jnp.bfloat16)
+    mix_high[...] = high
+    mix_low[...] = (shares - high.astype(jnp.float32)).astype(jnp.bfloat16)
+
+    def take_first(step, carry):
+        from_ = peer(step)
+        slot_copy(mine, from_[2]).wait_recv()
+        first_copy(mine, from_).wait_recv()
+        return carry
+
+    lax.fori_loop(1, n, take_first, 0)
+    stores = [
+        pltpu.make_async_copy(in_mats.at[0], gate_out.at[0], store_sem.at[0]),
+        pltpu.make_async_copy(in_mats.at[1], up_out.at[0], store_sem.at[1]),
+        pltpu.make_async_copy(out_mat, down_out.at[0], store_sem.at[2]),
+    ]
+    stores[0].start()
+    stores[1].start()
+
+    def activate(g, carry):
+        inputs = slots_in[pl.ds(g * group, group)].astype(jnp.float32)
+        inputs = inputs.reshape(group_rows, width).astype(jnp.bfloat16)
+        gate_pre = jnp.dot(inputs, in_mats[0], preferred_element_type=jnp.float32)
+        up_pre = jnp.dot(inputs, in_mats[1], preferred_element_type=jnp.float32)
+        gate_part = jnp.minimum(gate_pre, clamp_limit)
+        linear_part = jnp.clip(up_pre, -clamp_limit, clamp_limit)
+        active[g] = (
+            gate_part * jax.nn.sigmoid(sigmoid_slope * gate_part) * (linear_part + 1.0)
+        ).astype(jnp.bfloat16)
+        return carry
+
+    lax.fori_loop(0, groups, activate, 0)
+
+    def take_second(step, carry):
+        second_copy(mine, peer(step)).wait_recv()
+        return carry
+
+    lax.fori_loop(1, n, take_second, 0)
+    stores[2].start()
+    home = me // group
+
+    def project(c):
+        g = lax.rem(home + c, groups)
+        rows = jnp.dot(active[g], out_mat[...], preferred_element_type=jnp.float32)
+        rows_out[pl.ds(g * group, group)] = rows.reshape(group, capacity, width).astype(
+            jnp.bfloat16
+        )
+
+    def send_group(c):
+        g = lax.rem(home + c, groups)
+
+        def send_back(step, carry):
+            to = g * group + lax.rem(me + step, group)
+
+            @pl.when(to != me)
+            def _():
+                back_copy((to // n_tp, lax.rem(to, n_tp), to), me).start()
+
+            return carry
+
+        lax.fori_loop(0, group, send_back, 0)
+
+    project(0)
+
+    def return_group(c, carry):
+        project(c)
+        send_group(c - 1)
+        return carry
+
+    lax.fori_loop(1, groups, return_group, 0)
+    send_group(groups - 1)
+    rows_in[me] = rows_out[me]
+
+    def take_back(step, carry):
+        back_copy(mine, peer(step)[2]).wait_recv()
+        return carry
+
+    lax.fori_loop(1, n, take_back, 0)
+    block = 512
+
+    def mix(c, carry):
+        cols = pl.ds(pl.multiple_of(c * block, block), block)
+        rows = rows_in[:, :, cols].astype(jnp.float32).reshape(n * capacity, block)
+        rows = rows.astype(jnp.bfloat16)
+        total = jnp.dot(mix_high[...], rows, preferred_element_type=jnp.float32)
+        total = total + jnp.dot(mix_low[...], rows, preferred_element_type=jnp.float32)
+        mixed[:, cols] = total.astype(jnp.bfloat16)
+        return carry
+
+    lax.fori_loop(0, width // block, mix, 0)
+
+    def drain(step, carry):
+        to = peer(step)
+        slot_copy(to, me).wait_send()
+        first_copy(to, mine).wait_send()
+        second_copy(to, mine).wait_send()
+        back_copy(to, me).wait_send()
+        return carry
+
+    lax.fori_loop(1, n, drain, 0)
+    for store in stores:
+        store.wait()
+
+
+def direct_shards(
+    tokens, routes, route_weight, norm_gain, gate_weight, up_weight, down_weight
+):
+    n_fs, n_tp = lax.axis_size("fs"), lax.axis_size("tp")
+    n = n_fs * n_tp
+    tok_rows, width = tokens.shape
+    tile_rows, tile_cols = gate_weight.shape[1:]
+    down_rows, down_cols = down_weight.shape[1:]
+    hidden = n_tp * tile_cols
+    capacity = max(2, 3 * tok_rows * routes.shape[1] // (2 * n))
+    bf16, f32 = jnp.bfloat16, jnp.float32
+    whole = pl.BlockSpec(memory_space=pltpu.VMEM)
+    apart = pl.BlockSpec(memory_space=pl.ANY)
+    per_device = pltpu.SemaphoreType.DMA((n,))
+    return pl.pallas_call(
+        functools.partial(exchange_kernel, (n_fs, n_tp, capacity)),
+        out_shape=(
+            jax.ShapeDtypeStruct((1, width, hidden), bf16),
+            jax.ShapeDtypeStruct((1, width, hidden), bf16),
+            jax.ShapeDtypeStruct((1, hidden, width), bf16),
+            jax.ShapeDtypeStruct((tok_rows, width), bf16),
+        ),
+        in_specs=[whole] * 4 + [apart] * 3,
+        out_specs=(apart, apart, apart, whole),
+        scratch_shapes=[
+            pltpu.VMEM((n, tile_rows, tile_cols), f32),
+            pltpu.VMEM((n, tile_rows, tile_cols), f32),
+            pltpu.VMEM((n, down_rows, down_cols), f32),
+            pltpu.VMEM((n, 2, tile_rows, tile_cols), bf16),
+            pltpu.VMEM((n, down_rows, down_cols), bf16),
+            pltpu.VMEM((2, width, hidden), bf16),
+            pltpu.VMEM((hidden, width), bf16),
+            pltpu.VMEM((n, capacity, width), bf16),
+            pltpu.VMEM((n, capacity, width), bf16),
+            pltpu.VMEM((n // 8, 8 * capacity, hidden), bf16),
+            pltpu.VMEM((n, tok_rows), f32),
+            pltpu.VMEM((n * capacity, tok_rows), f32),
+            pltpu.VMEM((tok_rows, n * capacity), bf16),
+            pltpu.VMEM((tok_rows, n * capacity), bf16),
+            pltpu.VMEM((n, capacity, width), bf16),
+            pltpu.VMEM((n, capacity, width), bf16),
+            pltpu.SemaphoreType.DMA((3,)),
+            pltpu.SemaphoreType.DMA((3,)),
+        ]
+        + [per_device] * 8,
+        compiler_params=pltpu.CompilerParams(
+            collective_id=0, has_side_effects=True, vmem_limit_bytes=60 * 1024 * 1024
+        ),
+    )(
+        tokens,
+        routes.T,
+        route_weight.T,
+        norm_gain[:, None],
+        gate_weight,
+        up_weight,
+        down_weight,
+    )
+
+
+def aligned(mesh, tokens, routes, gate_weight, down_weight):
+    n_fs, n_tp = mesh.shape["fs"], mesh.shape["tp"]
+    n = n_fs * n_tp
+    tok_rows = tokens.shape[0] // n
+    capacity = max(2, 3 * tok_rows * routes.shape[1] // (2 * n))
+    return (
+        gate_weight.shape[0] == n
+        and n % 8 == 0
+        and capacity % 8 == 0
+        and tok_rows % 128 == 0
+        and tokens.shape[1] % 512 == 0
+        and gate_weight.shape[1] // n_fs % 16 == 0
+        and gate_weight.shape[2] // n_tp % 128 == 0
+        and down_weight.shape[1] // n_fs % 16 == 0
+        and down_weight.shape[2] // n_tp % 128 == 0
+    )
+
+
 def solution(mesh):
     placed = (
         P(("fs", "tp"), None),
@@ -89,15 +445,20 @@
         P(None, "fs", "tp"),
         P(None, "fs", "tp"),
     )
-    return jax.shard_map(
-        shards,
-        mesh=mesh,
-        in_specs=placed,
-        out_specs=(
-            P(("fs", "tp"), None, None),
-            P(("fs", "tp"), None, None),
-            P(("fs", "tp"), None, None),
-            P(("fs", "tp"), None),
-        ),
-        check_vma=False,
-    )
+
+    def run(tokens, routes, route_weight, norm_gain, gate_weight, up_weight, down_weight):
+        direct = aligned(mesh, tokens, routes, gate_weight, down_weight)
+        return jax.shard_map(
+            direct_shards if direct else shards,
+            mesh=mesh,
+            in_specs=placed,
+            out_specs=(
+                P(("fs", "tp"), None, None),
+                P(("fs", "tp"), None, None),
+                P(("fs", "tp"), None, None),
+                P(("fs", "tp"), None),
+            ),
+            check_vma=False,
+        )(tokens, routes, route_weight, norm_gain, gate_weight, up_weight, down_weight)
+
+    return run

time: 348 us -> 314 us (0.902)
  the two profiles are of different devices: /device:TPU:0 before, /device:TPU:29 now
where the time goes in v1:
time: 314 us; the launch traced here: 313 us
  Pallas kernels  303 us (96%)
  local copies, waits for them, and re-layouts  9.21 us (3%)
    pallas_call x1, Pallas kernels, direct_shards(): pl.pallas_call(functools.partial(exchange_kernel, (n_fs, n_tp, capacity))...  303 us
    unnamed x10, local copies, waits for them, and re-layouts  7.73 us

profile of v1, /device:TPU:29, one launch (start us, length us, event | category | flops | bytes accessed | tf_op | source)
XLA Modules:
  0.0 313.3 jit_solution(4533026933668679700)
XLA Ops:
  0.6 1.5 copy.11.gain
  2.1 303.4 %shard_map.102 = (bf16[1,2048,512]{2,1,0:T(8,128)(2,1)}, bf16[1,2048,512]{2,1,0:T(8,128)(2,1)}, bf16[1,512,2048]{2,1,0:T(8,128)(2,1)}, bf16[128,2048]{1,0:T(8,128)(2,1)}) custom-call(bf16[128,2048]{1,0:T(8,128)(2,1)} %tokens.1, s32[4,128]{1,0:T(4,128)} %bitcast.3, f32[4,128]{1,0:T(4,128)} %bitcast.4, f32[256,1]{1,0:T(8,128)} %copy.11.gain, ...), custom_call_target="tpu_custom_call" | custom-call | tf_op jit(solution)/shard_map/pallas_call | solution.py:375
  305.5 0.0 copy-start.1
  305.5 3.2 %copy.16 = bf16[1,2048,512]{2,1,0:T(8,128)(2,1)} copy(bf16[1,2048,512]{2,1,0:T(8,128)(2,1)} %get-tuple-element.8) | data formatting | bytes 4194304
  308.7 0.0 copy-done.1
  308.7 0.0 copy-start
  308.7 1.3 copy.17
  310.1 1.0 copy-done
  311.1 0.0 copy-start.2
  311.1 1.3 copy.18
  312.4 0.1 copy-done.2
  312.5 0.8 copy.19
Async XLA Ops:
  305.5 3.2 %copy-start.1 = (bf16[1,2048,512]{2,1,0:T(8,128)(2,1)S(1)}, bf16[1,2048,512]{2,1,0:T(8,128)(2,1)}, u32[]{:S(2)}) copy-start(bf16[1,2048,512]{2,1,0:T(8,128)(2,1)} %get-tuple-element.9) | copy-start | bytes 6291460
  308.7 2.3 copy-start
  311.1 1.4 copy-start.2

commit v2 on v1

--- a/solution.py
+++ b/solution.py
@@ -89,7 +89,8 @@
     gate_out, up_out, down_out, mixed,
     gate_in, up_in, down_in, in_tiles, out_tiles, in_mats, out_mat,
     slots_out, slots_in, active, ranks, picks, mix_high, mix_low, rows_out, rows_in,
-    load_sem, store_sem, slot_send, slot_recv, first_send, first_recv,
+    normed_out, normed_in, far_routes, far_weight, part_out, part_in,
+    trade_send, trade_recv, part_send, part_recv, load_sem, store_sem, slot_send, slot_recv, first_send, first_recv,
     second_send, second_recv, back_send, back_recv,
 ):
     n_fs, n_tp, capacity = sizes
@@ -103,9 +104,17 @@
     groups = n // group
     group_rows = group * capacity
 
+    half_fs, half_n = n_fs // 2, n // 2
+    half, place = fs // half_fs, lax.rem(fs, half_fs)
+    spot = place * n_tp + tp
+    half_groups = half_n // group
+    far = (lax.rem(fs + half_fs, n_fs), tp, lax.rem(me + half_n, n))
+
     def peer(step):
-        to_fs = lax.rem(fs + step // n_tp, n_fs)
-        to_tp = lax.rem(tp + lax.rem(step, n_tp), n_tp)
+        local = lax.rem(step + step // half_n, half_n)
+        side = lax.rem(half + 1 + step // half_n, 2)
+        to_fs = side * half_fs + lax.rem(place + local // n_tp, half_fs)
+        to_tp = lax.rem(tp + lax.rem(local, n_tp), n_tp)
         return to_fs, to_tp, to_fs * n_tp + to_tp
 
     barrier = pltpu.get_barrier_semaphore()
@@ -122,49 +131,80 @@
     ]
     for load in loads:
         load.start()
-    lax.fori_loop(1, n, greet, 0)
-
-    experts = lax.broadcasted_iota(jnp.int32, (n, tok_rows), 0)
-    named = jnp.zeros((n, tok_rows), jnp.float32)
-    scaled = jnp.zeros((n, tok_rows), jnp.float32)
-    for k in range(routes_t.shape[0]):
-        hit = routes_t[k : k + 1, :] == experts
-        named = named + hit.astype(jnp.float32)
-        scaled = scaled + jnp.where(hit, weight_t[k : k + 1, :], 0.0)
+    lax.fori_loop(0, n - 1, greet, 0)
+
     before = (
         lax.broadcasted_iota(jnp.int32, (tok_rows, tok_rows), 0)
         < lax.broadcasted_iota(jnp.int32, (tok_rows, tok_rows), 1)
     ).astype(jnp.float32).astype(jnp.bfloat16)
-    rank = jnp.dot(named.astype(jnp.bfloat16), before, preferred_element_type=jnp.float32)
-    ranks[...] = jnp.where(named > 0.5, rank, -1.0)
+    experts = lax.broadcasted_iota(jnp.int32, (half_n, tok_rows), 0) + half * half_n
+
+    def fill_slots(q, paths, shares, rows_ref):
+        named = jnp.zeros((half_n, tok_rows), jnp.float32)
+        scaled = jnp.zeros((half_n, tok_rows), jnp.float32)
+        for k in range(paths.shape[0]):
+            hit = paths[k : k + 1, :] == experts
+            named = named + hit.astype(jnp.float32)
+            scaled = scaled + jnp.where(hit, shares[k : k + 1, :], 0.0)
+        rank = jnp.dot(named.astype(jnp.bfloat16), before, preferred_element_type=jnp.float32)
+        ranks[q * half_n : (q + 1) * half_n, :] = jnp.where(named > 0.5, rank, -1.0)
+        number = lax.broadcasted_iota(jnp.int32, (group, capacity, tok_rows), 1).astype(jnp.float32)
+        for g in range(half_groups):
+            held = slice(q * half_n + g * group, q * half_n + (g + 1) * group)
+            select = (ranks[held, :][:, None, :] == number).astype(jnp.float32)
+            start = (q * half_groups + g) * group_rows
+            picks[start : start + group_rows, :] = (
+                select * scaled[g * group : (g + 1) * group, :][:, None, :]
+            ).reshape(group_rows, tok_rows)
+            rows = jnp.dot(
+                select.reshape(group_rows, tok_rows).astype(jnp.bfloat16),
+                rows_ref[...],
+                preferred_element_type=jnp.float32,
+            )
+            slots_out[held] = rows.reshape(group, capacity, width).astype(jnp.bfloat16)
+
     values = tokens[...].astype(jnp.float32)
     squares = jnp.mean(values * values, axis=1, keepdims=True)
-    normed = (values * lax.rsqrt(squares + norm_epsilon)).astype(jnp.bfloat16)
-    for g in range(groups):
-        held = slice(g * group, (g + 1) * group)
-        number = lax.broadcasted_iota(jnp.int32, (group, capacity, tok_rows), 1).astype(jnp.float32)
-        select = (ranks[held, :][:, None, :] == number).astype(jnp.float32)
-        picks[g * group_rows : (g + 1) * group_rows, :] = (
-            select * scaled[held, :][:, None, :]
-        ).reshape(group_rows, tok_rows)
-        rows = jnp.dot(
-            select.reshape(group_rows, tok_rows).astype(jnp.bfloat16),
-            normed,
-            preferred_element_type=jnp.float32,
-        )
-        slots_out[held] = rows.reshape(group, capacity, width).astype(jnp.bfloat16)
-
+    normed_out[...] = (values * lax.rsqrt(squares + norm_epsilon)).astype(jnp.bfloat16)
+
+    def trade(number, source, target):
+        return pltpu.make_async_remote_copy(
+            src_ref=source,
+            dst_ref=target,
+            send_sem=trade_send.at[number],
+            recv_sem=trade_recv.at[number],
+            device_id=(far[0], far[1]),
+            device_id_type=MESH,
+        )
+
+    trades = [
+        trade(0, routes_t, far_routes),
+        trade(1, weight_t, far_weight),
+        trade(2, normed_out, normed_in),
+    ]
     pl.semaphore_wait(barrier, n - 1)
-
-    def slot_copy(to, source):
+    for each in trades:
+        each.start()
+    fill_slots(0, routes_t, weight_t, normed_out)
+
+    def near(step):
+        to_place = lax.rem(place + step // n_tp, half_fs)
+        to_tp = lax.rem(tp + lax.rem(step, n_tp), n_tp)
+        return half * half_fs + to_place, to_tp, to_place * n_tp + to_tp
+
+    def slot_copy(q, to, source):
+        block = q * half_n + to[2]
         return pltpu.make_async_remote_copy(
-            src_ref=slots_out.at[to[2]],
+            src_ref=slots_out.at[block],
             dst_ref=slots_in.at[source],
-            send_sem=slot_send.at[to[2]],
+            send_sem=slot_send.at[block],
             recv_sem=slot_recv.at[source],
             device_id=(to[0], to[1]),
             device_id_type=MESH,
         )
+
+    def owner(q, at):
+        return lax.rem(half + q, 2) * half_n + at
 
     def first_copy(to, place):
         return pltpu.make_async_remote_copy(
@@ -193,24 +233,26 @@
             device_id_type=MESH,
         )
 
-    def back_copy(to, source):
+    def back_copy(source, block):
+        to_spot = lax.rem(source, half_n)
         return pltpu.make_async_remote_copy(
-            src_ref=rows_out.at[to[2]],
-            dst_ref=rows_in.at[source],
-            send_sem=back_send.at[to[2]],
-            recv_sem=back_recv.at[source],
-            device_id=(to[0], to[1]),
+            src_ref=rows_out.at[source],
+            dst_ref=rows_in.at[block],
+            send_sem=back_send.at[source],
+            recv_sem=back_recv.at[block],
+            device_id=(half * half_fs + to_spot // n_tp, lax.rem(to_spot, n_tp)),
             device_id_type=MESH,
         )
 
     mine = (fs, tp, me)
 
-    def send_slots(step, carry):
-        slot_copy(peer(step), me).start()
-        return carry
-
-    lax.fori_loop(1, n, send_slots, 0)
-    slots_in[me] = slots_out[me]
+    def send_slots(q):
+        def send_one(step, carry):
+            slot_copy(q, near(step), owner(q, spot)).start()
+            return carry
+
+        lax.fori_loop(1, half_n, send_one, 0)
+        slots_in[owner(q, spot)] = slots_out[q * half_n + spot]
 
     loads[0].wait()
     loads[1].wait()
@@ -221,14 +263,20 @@
         in_tiles[e, 0] = (gate_in[e] * gains).astype(jnp.bfloat16)
         in_tiles[e, 1] = (up_in[e] * gains).astype(jnp.bfloat16)
 
-    cast_first(1)
+    cast_first(0)
 
     def send_first(step, carry):
         cast_first(step + 1)
         first_copy(peer(step), mine).start()
         return carry
 
-    lax.fori_loop(1, n, send_first, 0)
+    lax.fori_loop(0, half_n, send_first, 0)
+    send_slots(0)
+    for each in trades:
+        each.wait_recv()
+    fill_slots(1, far_routes, far_weight, normed_in)
+    lax.fori_loop(half_n, n - 1, send_first, 0)
+    send_slots(1)
     own_rows = pl.ds(pl.multiple_of(fs * tile_rows, tile_rows), tile_rows)
     own_cols = pl.ds(pl.multiple_of(tp * tile_cols, tile_cols), tile_cols)
     in_mats[0, own_rows, own_cols] = in_tiles[me, 0]
@@ -240,14 +288,14 @@
         e = peer(step)[2]
         out_tiles[e] = down_in[e].astype(jnp.bfloat16)
 
-    cast_second(1)
+    cast_second(0)
 
     def send_second(step, carry):
         cast_second(step + 1)
         second_copy(peer(step), mine).start()
         return carry
 
-    lax.fori_loop(1, n, send_second, 0)
+    lax.fori_loop(0, n - 1, send_second, 0)
     out_mat[
         pl.ds(pl.multiple_of(fs * down_rows, down_rows), down_rows),
         pl.ds(pl.multiple_of(tp * down_cols, down_cols), down_cols),
@@ -258,13 +306,19 @@
     mix_high[...] = high
     mix_low[...] = (shares - high.astype(jnp.float32)).astype(jnp.bfloat16)
 
+    def take_slots(step, carry):
+        from_spot = near(step)[2]
+        for q in range(2):
+            slot_copy(q, near(step), owner(q, from_spot)).wait_recv()
+        return carry
+
+    lax.fori_loop(1, half_n, take_slots, 0)
+
     def take_first(step, carry):
-        from_ = peer(step)
-        slot_copy(mine, from_[2]).wait_recv()
-        first_copy(mine, from_).wait_recv()
-        return carry
-
-    lax.fori_loop(1, n, take_first, 0)
+        first_copy(mine, peer(step)).wait_recv()
+        return carry
+
+    lax.fori_loop(0, n - 1, take_first, 0)
     stores = [
         pltpu.make_async_copy(in_mats.at[0], gate_out.at[0], store_sem.at[0]),
         pltpu.make_async_copy(in_mats.at[1], up_out.at[0], store_sem.at[1]),
@@ -291,9 +345,9 @@
         second_copy(mine, peer(step)).wait_recv()
         return carry
 
-    lax.fori_loop(1, n, take_second, 0)
+    lax.fori_loop(0, n - 1, take_second, 0)
     stores[2].start()
-    home = me // group
+    home = (1 - half) * half_groups
 
     def project(c):
         g = lax.rem(home + c, groups)
@@ -306,11 +360,12 @@
         g = lax.rem(home + c, groups)
 
         def send_back(step, carry):
-            to = g * group + lax.rem(me + step, group)
-
-            @pl.when(to != me)
+            source = g * group + lax.rem(me + step, group)
+            crossing = lax.rem(source // half_n + half, 2)
+
+            @pl.when(lax.rem(source, half_n) != spot)
             def _():
-                back_copy((to // n_tp, lax.rem(to, n_tp), to), me).start()
+                back_copy(source, crossing * half_n + spot).start()
 
             return carry
 
@@ -325,35 +380,70 @@
 
     lax.fori_loop(1, groups, return_group, 0)
     send_group(groups - 1)
-    rows_in[me] = rows_out[me]
-
-    def take_back(step, carry):
-        back_copy(mine, peer(step)[2]).wait_recv()
-        return carry
-
-    lax.fori_loop(1, n, take_back, 0)
+    for q in range(2):
+        rows_in[q * half_n + spot] = rows_out[owner(q, spot)]
     block = 512
-
-    def mix(c, carry):
-        cols = pl.ds(pl.multiple_of(c * block, block), block)
-        rows = rows_in[:, :, cols].astype(jnp.float32).reshape(n * capacity, block)
-        rows = rows.astype(jnp.bfloat16)
-        total = jnp.dot(mix_high[...], rows, preferred_element_type=jnp.float32)
-        total = total + jnp.dot(mix_low[...], rows, preferred_element_type=jnp.float32)
-        mixed[:, cols] = total.astype(jnp.bfloat16)
-        return carry
-
-    lax.fori_loop(0, width // block, mix, 0)
+    span = half_n * capacity
+
+    def combine(q, cols):
+        rows = rows_in[q * half_n : (q + 1) * half_n, :, cols].astype(jnp.float32)
+        rows = rows.reshape(span, block).astype(jnp.bfloat16)
+        taken = slice(q * span, (q + 1) * span)
+        total = jnp.dot(mix_high[:, taken], rows, preferred_element_type=jnp.float32)
+        return total + jnp.dot(mix_low[:, taken], rows, preferred_element_type=jnp.float32)
+
+    def take_back(q):
+        def take_one(step, carry):
+            back_copy(owner(q, spot), q * half_n + near(step)[2]).wait_recv()
+            return carry
+
+        lax.fori_loop(1, half_n, take_one, 0)
+
+    def part_copy(c):
+        cols = slice(c * block, (c + 1) * block)
+        return pltpu.make_async_remote_copy(
+            src_ref=part_out.at[:, cols],
+            dst_ref=part_in.at[:, cols],
+            send_sem=part_send.at[c],
+            recv_sem=part_recv.at[c],
+            device_id=(far[0], far[1]),
+            device_id_type=MESH,
+        )
+
+    take_back(1)
+    for c in range(width // block):
+        cols = slice(c * block, (c + 1) * block)
+        part_out[:, cols] = combine(1, cols).astype(jnp.bfloat16)
+        if c > 0:
+            part_copy(c - 1).start()
+    part_copy(width // block - 1).start()
+    take_back(0)
+    for c in range(width // block):
+        cols = slice(c * block, (c + 1) * block)
+        total = combine(0, cols)
+        part_copy(c).wait_recv()
+        mixed[:, cols] = (total + part_in[:, cols].astype(jnp.float32)).astype(jnp.bfloat16)
 
     def drain(step, carry):
         to = peer(step)
-        slot_copy(to, me).wait_send()
         first_copy(to, mine).wait_send()
         second_copy(to, mine).wait_send()
-        back_copy(to, me).wait_send()
-        return carry
-
-    lax.fori_loop(1, n, drain, 0)
+        return carry
+
+    lax.fori_loop(0, n - 1, drain, 0)
+
+    def drain_near(step, carry):
+        to = near(step)
+        for q in range(2):
+            slot_copy(q, to, owner(q, spot)).wait_send()
+            back_copy(owner(q, to[2]), q * half_n + spot).wait_send()
+        return carry
+
+    lax.fori_loop(1, half_n, drain_near, 0)
+    for each in trades:
+        each.wait_send()
+    for c in range(width // block):
+        part_copy(c).wait_send()
     for store in stores:
         store.wait()
 
@@ -399,6 +489,16 @@
             pltpu.VMEM((tok_rows, n * capacity), bf16),
             pltpu.VMEM((n, capacity, width), bf16),
             pltpu.VMEM((n, capacity, width), bf16),
+            pltpu.VMEM((tok_rows, width), bf16),
+            pltpu.VMEM((tok_rows, width), bf16),
+            pltpu.VMEM((routes.shape[1], tok_rows), routes.dtype),
+            pltpu.VMEM((routes.shape[1], tok_rows), f32),
+            pltpu.VMEM((tok_rows, width), bf16),
+            pltpu.VMEM((tok_rows, width), bf16),
+            pltpu.SemaphoreType.DMA((3,)),
+            pltpu.SemaphoreType.DMA((3,)),
+            pltpu.SemaphoreType.DMA((width // 512,)),
+            pltpu.SemaphoreType.DMA((width // 512,)),
             pltpu.SemaphoreType.DMA((3,)),
             pltpu.SemaphoreType.DMA((3,)),
         ]
@@ -424,7 +524,8 @@
     capacity = max(2, 3 * tok_rows * routes.shape[1] // (2 * n))
     return (
         gate_weight.shape[0] == n
-        and n % 8 == 0
+        and n_fs % 2 == 0
+        and n % 16 == 0
         and capacity % 8 == 0
         and tok_rows % 128 == 0
         and tokens.shape[1] % 512 == 0

time: 314 us -> 241 us (0.77)
  the two profiles are of different devices: /device:TPU:29 before, /device:TPU:0 now
where the time goes in v2:
time: 241 us; the launch traced here: 240 us
  Pallas kernels  230 us (95%)
  local copies, waits for them, and re-layouts  9.21 us (4%)
    pallas_call x1, Pallas kernels, direct_shards(): pl.pallas_call(functools.partial(exchange_kernel, (n_fs, n_tp, capacity))...  230 us
    unnamed x10, local copies, waits for them, and re-layouts  7.73 us

profile of v2, /device:TPU:0, one launch (start us, length us, event | category | flops | bytes accessed | tf_op | source)
XLA Modules:
  0.0 240.1 jit_solution(11012417877655915344)
XLA Ops:
  0.6 1.5 copy.11.gain
  2.1 230.3 %shard_map.102 = (bf16[1,2048,512]{2,1,0:T(8,128)(2,1)}, bf16[1,2048,512]{2,1,0:T(8,128)(2,1)}, bf16[1,512,2048]{2,1,0:T(8,128)(2,1)}, bf16[128,2048]{1,0:T(8,128)(2,1)}) custom-call(bf16[128,2048]{1,0:T(8,128)(2,1)} %tokens.1, s32[4,128]{1,0:T(4,128)} %bitcast.3, f32[4,128]{1,0:T(4,128)} %bitcast.4, f32[256,1]{1,0:T(8,128)} %copy.11.gain, ...), custom_call_target="tpu_custom_call" | custom-call | tf_op jit(solution)/shard_map/pallas_call | solution.py:465
  232.4 0.0 copy-start.1
  232.4 3.2 %copy.16 = bf16[1,2048,512]{2,1,0:T(8,128)(2,1)} copy(bf16[1,2048,512]{2,1,0:T(8,128)(2,1)} %get-tuple-element.8) | data formatting | bytes 4194304
  235.6 0.0 copy-done.1
  235.6 0.0 copy-start
  235.6 1.3 copy.17
  236.9 1.0 copy-done
  237.9 0.0 copy-start.2
  237.9 1.3 copy.18
  239.2 0.1 copy-done.2
  239.3 0.8 copy.19
Async XLA Ops:
  232.4 3.2 %copy-start.1 = (bf16[1,2048,512]{2,1,0:T(8,128)(2,1)S(1)}, bf16[1,2048,512]{2,1,0:T(8,128)(2,1)}, u32[]{:S(2)}) copy-start(bf16[1,2048,512]{2,1,0:T(8,128)(2,1)} %get-tuple-element.9) | copy-start | bytes 6291460
  235.6 2.3 copy-start
  237.9 1.4 copy-start.2
